TPU v7x, 32 devices: a whole 2x2x4 slice. The times are simulated.
32 devices in a mesh: sp: 8 (over z, y), tp: 4 (over x, core).
Axes of the slice: x: 2, y: 2, z: 4, core: 2. Of those that a mesh axis runs over, the one named last changes fastest.
Arguments:
- stream: bfloat16 [1536, 2048], P('sp'), may hold values from -6 to 6
- upstream: bfloat16 [1536, 2048], P('sp'), may hold values from -6 to 6
- expert_gain: float32 [2048], replicated, may hold values from 0.1 to 1.9
- expert_ids: int32 [1536, 2], P('sp'), may hold values from 0 to 7, all different within a row; in each aligned block of 192 rows (0 to 191, 192 to 383, ...) at most 60 rows name the same one
- group_weight: float32 [1536], P('sp'), may hold values from 0.25 to 1
- pair_scores: float32 [1536, 2], P('sp'), may hold values from -6 to 6
- gate_weight: bfloat16 [8, 2048, 1024], P('sp', None, 'tp'), may hold values from -0.125 to 0.125
- up_weight: bfloat16 [8, 2048, 1024], P('sp', None, 'tp'), may hold values from -0.125 to 0.125
- down_weight: bfloat16 [8, 1024, 2048], P('sp', 'tp'), may hold values from -0.1875 to 0.1875
- mixer_weight: bfloat16 [1024, 2048], P('tp'), may hold values from -0.1875 to 0.1875
- filtered: bfloat16 [1536, 1024], P('sp', 'tp'), may hold values from -1000 to 1000
- channel_gain: float32 [1024], P('tp'), may hold values from 0.1 to 1.9
- kernel_taps: float32 [31, 1024], P(None, 'tp'), may hold values from -1 to 1
- value_branch: bfloat16 [1536, 1024], P('sp', 'tp'), may hold values from -6 to 6
- gate_branch: bfloat16 [1536, 1024], P('sp', 'tp'), may hold values from -6 to 6
Outputs:
- gradient_value: bfloat16 [1536, 1024], P('sp', 'tp')
- gradient_gating: bfloat16 [1536, 1024], P('sp', 'tp')
- gradient_mixer: float32 [2048, 1024], P('sp', 'tp')
- gradient_gate: float32 [8, 2048, 1024], P('sp', None, 'tp')
- gradient_up: float32 [8, 2048, 1024], P('sp', None, 'tp')
- gradient_down: float32 [8, 1024, 2048], P('sp', 'tp')
Inputs may be any that keep to these rules, and one draw needn't show every extreme that they name: `expert_ids`: the two experts of a token differ. Among the rows of one index of sp, at most 60 routes name the same expert, and in every draw some expert is named by exactly 60 of them.
All inputs are finite; a program needn't handle non-finite values.
Results may differ from a plain program's by a relative error of at most 0.012.
Values may be sent and summed in bfloat16 or wider, within the bound.
A program may use at most 64 MiB of HBM per device.

v0:
```python
import jax
import jax.numpy as jnp
from jax import lax
from jax.sharding import PartitionSpec as P

EPS = 1e-06


def shifted(block, axis, distance):
    devices = range(lax.axis_size(axis))
    route = [(i - distance, i) for i in devices if i - distance in devices]
    return lax.ppermute(block, axis, route)


def route_slots(routes, capacity, experts):
    flat = routes.reshape(-1)
    onehot = (flat[:, None] == jnp.arange(experts, dtype=jnp.int32)[None, :]).astype(jnp.int32)
    before = jnp.cumsum(onehot, axis=0) - onehot
    position = jnp.sum(before * onehot, axis=1)
    slots = flat * capacity + position
    total = flat.shape[0]
    source = (
        jnp.full((experts * capacity,), total, jnp.int32)
        .at[slots]
        .set(jnp.arange(total, dtype=jnp.int32))
    )
    return (slots, source)


def silu_slope(value, sigma):
    return sigma * (1.0 + value * (1.0 - sigma))


def pack_routes(normed, scaled, source, experts, capacity):
    total = scaled.shape[0]
    token_index = jnp.where(source < total, source // 2, normed.shape[0])
    normed_ext = jnp.concatenate([normed, jnp.zeros((1, normed.shape[1]), normed.dtype)], axis=0)
    scaled_ext = jnp.concatenate([scaled, jnp.zeros((1, scaled.shape[1]), scaled.dtype)], axis=0)
    return (
        normed_ext[token_index].reshape(experts, capacity, -1),
        scaled_ext[source].reshape(experts, capacity, -1),
    )


def contract_last(left, right):
    return lax.dot_general(
        left, right, (((1,), (1,)), ((), ())), preferred_element_type=jnp.float32
    )


def contract_first(left, right):
    return lax.dot_general(
        left, right, (((0,), (0,)), ((), ())), preferred_element_type=jnp.float32
    )


def body(
    stream,
    upstream,
    expert_gain,
    expert_ids,
    group_weight,
    pair_scores,
    gate_weight,
    up_weight,
    down_weight,
    mixer_weight,
    filtered,
    channel_gain,
    kernel_taps,
    value_branch,
    gate_branch,
):
    experts = lax.axis_size("sp")
    tokens_here, width = stream.shape
    capacity = max(2, 5 * tokens_here // (2 * experts))
    groups = lax.axis_size("tp")
    column = width // groups
    first_col = lax.axis_index("tp") * column
    stream_f = stream.astype(jnp.float32)
    inv_rms = lax.rsqrt(jnp.mean(stream_f * stream_f, axis=1, keepdims=True) + EPS)
    normed = (stream_f * inv_rms * expert_gain).astype(jnp.bfloat16)
    spread = pair_scores[:, 0] - pair_scores[:, 1]
    route_weight = group_weight[:, None] * jnp.stack(
        [jax.nn.sigmoid(spread), jax.nn.sigmoid(-spread)], axis=1
    )
    scaled = (
        (route_weight[:, :, None] * upstream.astype(jnp.float32)[:, None, :])
        .astype(jnp.bfloat16)
        .reshape(2 * tokens_here, width)
    )
    slots, source = route_slots(expert_ids, capacity, experts)
    normed_part = lax.dynamic_slice_in_dim(normed, first_col, column, 1)
    scaled_part = lax.dynamic_slice_in_dim(scaled, first_col, column, 1)
    send_rows, send_cots = pack_routes(normed_part, scaled_part, source, experts, capacity)
    got_rows, got_cots = (
        lax.all_to_all(send_rows, "sp", split_axis=0, concat_axis=0, tiled=True),
        lax.all_to_all(send_cots, "sp", split_axis=0, concat_axis=0, tiled=True),
    )
    got_rows, got_cots = (
        lax.all_gather(got_rows, "tp", axis=2, tiled=True),
        lax.all_gather(got_cots, "tp", axis=2, tiled=True),
    )
    rows = got_rows.reshape(experts * capacity, width)
    cots = got_cots.reshape(experts * capacity, width)
    gate_local = gate_weight[0]
    up_local = up_weight[0]
    down_local = down_weight[0]
    pre_gate = jnp.dot(rows, gate_local, preferred_element_type=jnp.float32)
    pre_up = jnp.dot(rows, up_local, preferred_element_type=jnp.float32)
    sigma = jax.nn.sigmoid(pre_gate)
    silu_gate = pre_gate * sigma
    hidden = (silu_gate * pre_up).astype(jnp.bfloat16)
    grad_hidden = contract_last(cots, down_local)
    grad_pre_gate = (grad_hidden * pre_up * silu_slope(pre_gate, sigma)).astype(jnp.bfloat16)
    grad_pre_up = (grad_hidden * silu_gate).astype(jnp.bfloat16)
    partial_rows = contract_last(grad_pre_gate, gate_local) + contract_last(grad_pre_up, up_local)
    shared = lax.psum_scatter(
        partial_rows.astype(jnp.bfloat16), "tp", scatter_dimension=1, tiled=True
    )
    back = lax.all_to_all(
        shared.reshape(experts, capacity, column), "sp", split_axis=0, concat_axis=0, tiled=True
    )
    back = lax.all_gather(back, "tp", axis=2, tiled=True)
    gradient_gate = contract_first(rows, grad_pre_gate)[None]
    gradient_up = contract_first(rows, grad_pre_up)[None]
    gradient_down = contract_first(hidden, cots)[None]
    back_flat = back.reshape(experts * capacity, width)
    per_route = back_flat[slots].astype(jnp.float32).reshape(tokens_here, 2, width)
    grad_normed = per_route[:, 0] + per_route[:, 1]
    weighted = grad_normed * expert_gain
    inner = jnp.mean(weighted * stream_f, axis=1, keepdims=True)
    grad_stream = (
        upstream.astype(jnp.float32)
        + inv_rms * weighted
        - stream_f * inv_rms * inv_rms * inv_rms * inner
    ).astype(jnp.bfloat16)
    grad_act = contract_last(grad_stream, mixer_weight)
    filt = filtered.astype(jnp.float32)
    channels = filt.shape[1] * groups
    total_sum, total_square = lax.psum((jnp.sum(filt, axis=1), jnp.sum(filt * filt, axis=1)), "tp")
    mean_c = total_sum[:, None] / channels
    variance = total_square[:, None] / channels - mean_c * mean_c
    inv_std = lax.rsqrt(variance + EPS)
    centred = (filt - mean_c) * inv_std
    normal_out = centred * channel_gain
    sig_norm = jax.nn.sigmoid(normal_out)
    activated = (normal_out * sig_norm).astype(jnp.bfloat16)
    grad_centred = grad_act * silu_slope(normal_out, sig_norm) * channel_gain
    slope_sum, slope_cross = lax.psum(
        (jnp.sum(grad_centred, axis=1), jnp.sum(grad_centred * centred, axis=1)), "tp"
    )
    grad_filtered = (
        inv_std
        * (grad_centred - slope_sum[:, None] / channels - centred * slope_cross[:, None] / channels)
    ).astype(jnp.bfloat16)
    reach = kernel_taps.shape[0] - 1
    ahead = shifted(grad_filtered[:reach], "sp", -1)
    extended = jnp.concatenate([grad_filtered, ahead], axis=0).astype(jnp.float32)
    grad_mixed = lax.conv_general_dilated(
        extended[None],
        kernel_taps[::-1][:, None, :],
        (1,),
        "VALID",
        dimension_numbers=("NWC", "WIO", "NWC"),
        feature_group_count=filt.shape[1],
        precision=lax.Precision.HIGHEST,
    )[0]
    sig_gate = jax.nn.sigmoid(gate_branch.astype(jnp.float32))
    gradient_value = (grad_mixed * sig_gate).astype(jnp.bfloat16)
    gradient_gating = (
        grad_mixed * value_branch.astype(jnp.float32) * sig_gate * (1.0 - sig_gate)
    ).astype(jnp.bfloat16)
    gradient_mixer = lax.psum_scatter(
        contract_first(grad_stream, activated), "sp", scatter_dimension=0, tiled=True
    )
    return (
        gradient_value,
        gradient_gating,
        gradient_mixer,
        gradient_gate,
        gradient_up,
        gradient_down,
    )


def solution(mesh):
    return jax.shard_map(
        body,
        mesh=mesh,
        in_specs=(
            P("sp", None),
            P("sp", None),
            P(),
            P("sp", None),
            P("sp"),
            P("sp", None),
            P("sp", None, "tp"),
            P("sp", None, "tp"),
            P("sp", "tp", None),
            P("tp", None),
            P("sp", "tp"),
            P("tp"),
            P(None, "tp"),
            P("sp", "tp"),
            P("sp", "tp"),
        ),
        out_specs=(
            P("sp", "tp"),
            P("sp", "tp"),
            P("sp", "tp"),
            P("sp", None, "tp"),
            P("sp", None, "tp"),
            P("sp", "tp", None),
        ),
        check_vma=False,
    )
```

profile of v0, /device:TPU:0, one launch (start us, length us, event | category | flops | bytes accessed | tf_op | source)
XLA Modules:
  0.0 268.8 jit_solution(1533650336860865618)
XLA Ops:
  7.2 0.9 copy.25
  8.1 0.1 eq.29
  8.3 0.1 eq.25
  8.4 0.7 broadcast_multiply_fusion
  9.1 1.4 fusion
  10.5 1.3 convert_multiply_fusion.1
  11.8 0.9 reduce-window.6
  12.7 0.2 slice_reduce_fusion
  12.9 0.1 copy.24
  13.1 0.1 mul.216
  13.2 0.1 fusion.51
  13.3 2.9 %scatter_custom_fusion = s32[480]{0:T(512)S(1)} fusion(s32[384]{0:T(512)S(1)} %fusion.56, s32[384]{0:T(512)S(1)} %iota.11, s32[]{:T(128)} %constant.56.clone.1), kind=kCustom, calls=%fused_computation.99 | custom fusion | bytes 1924 | tf_op jit(solution)/shard_map/scatter | solution.py:25
  16.3 0.1 dynamic-slice
  16.4 2.1 gather_fusion.1
  18.6 0.1 reshape.138
  18.7 21.9 %all_to_all.15 = bf16[8,60,512]{2,1,0:T(8,128)(2,1)} all-to-all(bf16[8,60,512]{2,1,0:T(8,128)(2,1)S(1)} %reshape.138), channel_id=1, replica_groups=mesh['sp'=8,'tp'=4] {'sp'}, dimensions={0} | all-to-all | bytes 983040 | tf_op jit(solution)/shard_map/all_to_all | solution.py:97
  40.6 0.0 all-gather.4.cloned.1.call-start
  40.7 0.1 copy.23
  40.8 0.1 stack.14
  41.0 0.1 mul.206
  41.1 0.1 mul.207
  41.2 3.2 %mul.210 = f32[192,2,2048]{2,1,0:T(2,128)} broadcast(bf16[192,2048]{1,0:T(8,128)(2,1)S(1)} %copy-done.4), dimensions={0,2} | broadcast | bytes 3932160 | tf_op jit(solution)/shard_map/mul | solution.py:88
  44.5 5.6 %mul.211 = f32[384,2048]{1,0:T(8,128)} reshape(f32[192,2,2048]{2,1,0:T(2,128)} %mul.210) | data formatting | bytes 6291456 | tf_op jit(solution)/shard_map/mul | solution.py:88
  50.1 1.2 fusion.14
  51.4 2.1 gather_fusion
  53.5 0.1 reshape.136
  53.6 17.4 %all_to_all.16 = bf16[8,60,512]{2,1,0:T(8,128)(2,1)} all-to-all(bf16[8,60,512]{2,1,0:T(8,128)(2,1)S(1)} %reshape.136), channel_id=1, replica_groups=mesh['sp'=8,'tp'=4] {'sp'}, dimensions={0} | all-to-all | bytes 983040 | tf_op jit(solution)/shard_map/all_to_all | solution.py:98
  71.0 0.0 reduce-scatter.3.cloned.1.call-start
  71.0 1.7 reshape.139
  72.8 2.6 fusion.10
  75.4 1.5 fusion.7
  76.9 15.8 %all-gather.4.cloned.1.call-done = bf16[8,60,2048]{2,1,0:T(8,128)(2,1)} async-done(((bf16[8,60,512]{2,1,0:T(8,128)(2,1)}), bf16[8,60,2048]{2,1,0:T(8,128)(2,1)}) %all-gather.4.cloned.1.call-update) | async-done | bytes 1966096 | tf_op jit(solution)/shard_map/all_gather | solution.py:102
  92.7 1.7 reshape.137
  94.5 2.8 %multiply_convert_fusion.1 = (bf16[480,256]{1,0:T(8,128)(2,1)S(1)}, bf16[480,256]{1,0:T(8,128)(2,1)S(1)}) fusion(f32[480,256]{1,0:T(8,128)} %fusion.7, f32[480,256]{1,0:T(8,128)S(1)} %fusion.10, bf16[480,2048]{1,0:T(8,128)(2,1)S(1)} %reshape.137, bf16[1,256,2048]{2,1,0:T(8,128)(2,1)} %param.23), kind=kOutput, calls=%fused_computation.31 | convolution fusion | flops 504913920 | bytes 4489216 | tf_op jit(solution)/shard_map/dot_general | solution.py:46
  97.4 0.7 fusion.5
  98.1 0.6 copy-done.7
  98.8 2.0 add_convert_fusion
  100.8 0.0 all-gather.8.cloned.1.call-start
  100.8 30.5 %reduce-scatter.3.cloned.1.call-done = bf16[480,512]{1,0:T(8,128)(2,1)} async-done(((bf16[480,2048]{1,0:T(8,128)(2,1)}), bf16[480,512]{1,0:T(8,128)(2,1)}) %reduce-scatter.3.cloned.1.call-update) | async-done | bytes 491536 | tf_op jit(solution)/shard_map/reduce_scatter | solution.py:118
  131.3 1.1 reshape.140
  132.4 19.8 %all_to_all.17 = bf16[8,60,512]{2,1,0:T(8,128)(2,1)} all-to-all(bf16[8,60,512]{2,1,0:T(8,128)(2,1)S(1)} %reshape.140), channel_id=1, replica_groups=mesh['sp'=8,'tp'=4] {'sp'}, dimensions={0} | all-to-all | bytes 983040 | tf_op jit(solution)/shard_map/all_to_all | solution.py:121
  152.3 0.2 fusion.19
  152.5 6.1 %all-reduce.3 = (f32[192]{0:T(256)S(1)}, f32[192]{0:T(256)S(1)}) all-reduce(f32[192]{0:T(256)S(1)} %get-tuple-element.9, f32[192]{0:T(256)S(1)} %get-tuple-element.8), channel_id=1, replica_groups=mesh['sp'=8,'tp'=4] {'tp'}, use_global_device_ids=true, to_apply=%region_3.4 | all-reduce | flops 384 | bytes 3072 | tf_op jit(solution)/shard_map/psum | solution.py:141
  158.6 14.4 %all-gather.8.cloned.1.call-done = bf16[8,60,2048]{2,1,0:T(8,128)(2,1)} async-done(((bf16[8,60,512]{2,1,0:T(8,128)(2,1)}), bf16[8,60,2048]{2,1,0:T(8,128)(2,1)}) %all-gather.8.cloned.1.call-update) | async-done | bytes 1966096 | tf_op jit(solution)/shard_map/all_gather | solution.py:124
  173.0 1.7 reshape.141
  174.8 3.1 %gather_fusion.2 = bf16[384,2048]{1,0:T(8,128)(2,1)} fusion(bf16[480,2048]{1,0:T(8,128)(2,1)S(1)} %reshape.141, s32[1024]{0:T(1024)S(1)} %pad_clamp_fusion), kind=kCustom, calls=%fused_computation.2 | custom fusion | bytes 3147264 | tf_op jit(solution)/shard_map/gather | solution.py:129
  177.9 4.7 %reshape.142 = f32[192,2,2048]{2,1,0:T(2,128)} reshape(bf16[384,2048]{1,0:T(8,128)(2,1)} %gather_fusion.2) | data formatting | bytes 4718592 | tf_op jit(solution)/shard_map/convert_element_type | solution.py:129
  182.6 6.1 %fusion.62 = (f32[192,1,2048]{2,1,0:T(1,128)S(1)}, f32[192,1,2048]{2,1,0:T(1,128)S(1)}) fusion(f32[192,2,2048]{2,1,0:T(2,128)} %reshape.142), kind=kLoop, calls=%fused_computation.112 | loop fusion | bytes 6291456 | tf_op jit(solution)/shard_map/slice | solution.py:130
  188.8 1.0 fusion.1
  189.8 0.1 copy-done.5
  189.9 1.9 subtract_convert_fusion
  191.8 1.9 fusion.42
  193.8 0.1 rev.3
  193.9 3.8 %convolution_bitcast_fusion.1 = f32[1,2048,256]{2,1,0:T(8,128)} fusion(bf16[480,2048]{1,0:T(8,128)(2,1)} %copy-done.6, bf16[480,256]{1,0:T(8,128)(2,1)S(1)} %copy-done.13), kind=kOutput, calls=%fused_computation.6 | convolution fusion | flops 503316480 | bytes 4308992 | tf_op jit(solution)/shard_map/dot_general | solution.py:52
  197.7 2.1 convolution_bitcast_fusion
  199.8 0.6 fusion.61
  200.5 6.3 %all-reduce.2 = (f32[192]{0:T(256)S(1)}, f32[192]{0:T(256)S(1)}) all-reduce(f32[192]{0:T(256)S(1)} %get-tuple-element.7, f32[192]{0:T(256)S(1)} %get-tuple-element.6), channel_id=1, replica_groups=mesh['sp'=8,'tp'=4] {'tp'}, use_global_device_ids=true, to_apply=%region_14.15 | all-reduce | flops 384 | bytes 3072 | tf_op jit(solution)/shard_map/psum | solution.py:150
  206.8 0.2 fusion.37
  206.9 1.3 collective-permute-start
  208.3 3.6 %convolution_bitcast_fusion.2 = f32[1,2048,256]{2,1,0:T(8,128)} fusion(bf16[480,2048]{1,0:T(8,128)(2,1)} %copy-done.6, bf16[480,256]{1,0:T(8,128)(2,1)S(1)} %copy-done.15), kind=kOutput, calls=%fused_computation.7 | convolution fusion | flops 503316480 | bytes 4308992 | tf_op jit(solution)/shard_map/dot_general | solution.py:52
  211.9 0.7 collective-permute-done
  212.6 2.9 %fusion.17 = f32[1,192,256]{2,0,1:T(1,128)S(1)} fusion(bf16[1,222,256]{2,1,0:T(8,128)(2,1)S(1)} %maximum_bitcast_fusion, f32[31,1,256]{2,0,1:T(8,128)S(1)} %bitcast.71), kind=kOutput, calls=%fused_computation.40 | convolution fusion | flops 18284544 | bytes 342016 | tf_op jit(solution)/shard_map/conv_general_dilated | solution.py:160
  215.5 0.8 fusion.41
  216.2 46.0 %reduce-scatter.5.cloned.1.call-done = f32[256,256]{1,0:T(8,128)} async-done(((f32[2048,256]{1,0:T(8,128)}), f32[256,256]{1,0:T(8,128)}) %reduce-scatter.5.cloned.1.call-update) | async-done | bytes 262160 | tf_op jit(solution)/shard_map/reduce_scatter | solution.py:174
  (74 shorter events, 0.6 us)
Async XLA Ops:
  7.2 68.3 %copy-start = (bf16[1,2048,256]{2,1,0:T(8,128)(2,1)S(1)}, bf16[1,2048,256]{2,1,0:T(8,128)(2,1)}, u32[]{:S(2)}) copy-start(bf16[1,2048,256]{2,1,0:T(8,128)(2,1)} %param.21) | copy-start | bytes 3145732
  7.2 9.1 %copy-start.18 = (f32[2048]{0:T(1024)S(1)}, f32[2048]{0:T(1024)}, u32[]{:S(2)}) copy-start(f32[2048]{0:T(1024)} %param.17) | copy-start | bytes 24580
  7.2 63.8 %all-gather.6.cloned.1.call-start = ((), (), s32[]{:S(2)}) async-start(), calls=%async_computation.6 | async-start | bytes 2621440 | tf_op jit(solution)/shard_map/all_gather | solution.py:101
  18.6 22.1 %copy-start.20 = (f32[192,2]{0,1:T(2,128)S(1)}, f32[192,2]{0,1:T(2,128)}, u32[]{:S(2)}) copy-start(f32[192,2]{0,1:T(2,128)} %param.20) | copy-start | bytes 4612
  18.6 22.4 %copy-start.21 = (f32[192]{0:T(256)S(1)}, f32[192]{0:T(256)}, u32[]{:S(2)}) copy-start(f32[192]{0:T(256)} %param.19) | copy-start | bytes 2308
  18.6 22.6 %copy-start.4 = (bf16[192,2048]{1,0:T(8,128)(2,1)S(1)}, bf16[192,2048]{1,0:T(8,128)(2,1)}, u32[]{:S(2)}) copy-start(bf16[192,2048]{1,0:T(8,128)(2,1)} %param.16) | copy-start | bytes 2359300
  40.6 52.1 %all-gather.4.cloned.1.call-start = ((), (), s32[]{:S(2)}) async-start(), calls=%async_computation.5 | async-start | bytes 2621440 | tf_op jit(solution)/shard_map/all_gather | solution.py:102
  71.0 60.4 %reduce-scatter.3.cloned.1.call-start = ((), (), s32[]{:S(2)}) async-start(), calls=%async_computation.7 | async-start | bytes 2457600 | tf_op jit(solution)/shard_map/reduce_scatter | solution.py:118
  72.8 4.1 %copy-start.6 = (bf16[480,2048]{1,0:T(8,128)(2,1)}, bf16[480,2048]{1,0:T(8,128)(2,1)S(1)}, u32[]{:S(2)}) copy-start(bf16[480,2048]{1,0:T(8,128)(2,1)S(1)} %reshape.139) | copy-start | bytes 5898244
  75.4 19.1 %copy-start.9 = (f32[480,256]{1,0:T(8,128)}, f32[480,256]{1,0:T(8,128)S(1)}, u32[]{:S(2)}) copy-start(f32[480,256]{1,0:T(8,128)S(1)} %fusion.10) | copy-start | bytes 1474564
  94.5 2.8 %copy-start.2 = (bf16[480,2048]{1,0:T(8,128)(2,1)}, bf16[480,2048]{1,0:T(8,128)(2,1)S(1)}, u32[]{:S(2)}) copy-start(bf16[480,2048]{1,0:T(8,128)(2,1)S(1)} %reshape.137) | copy-start | bytes 5898244
  97.4 0.8 copy-start.14
  97.4 0.8 copy-start.12
  97.4 1.4 copy-start.7
  100.8 51.5 %copy-start.8 = (bf16[192,256]{1,0:T(8,128)(2,1)S(1)}, bf16[192,256]{1,0:T(8,128)(2,1)}, u32[]{:S(2)}) copy-start(bf16[192,256]{1,0:T(8,128)(2,1)} %param.25) | copy-start | bytes 294916
  100.8 72.3 %all-gather.8.cloned.1.call-start = ((), (), s32[]{:S(2)}) async-start(), calls=%async_computation.8 | async-start | bytes 2621440 | tf_op jit(solution)/shard_map/all_gather | solution.py:124
  152.3 110.0 %reduce-scatter.5.cloned.1.call-start = ((), (), s32[]{:S(2)}) async-start(), calls=%async_computation.9 | async-start | bytes 2359296 | tf_op jit(solution)/shard_map/reduce_scatter | solution.py:174
  182.6 6.1 %copy-start.1 = (bf16[192,2048]{1,0:T(8,128)(2,1)S(1)}, bf16[192,2048]{1,0:T(8,128)(2,1)}, u32[]{:S(2)}) copy-start(bf16[192,2048]{1,0:T(8,128)(2,1)} %param.15) | copy-start | bytes 2359300
  188.8 1.1 copy-start.5
  189.9 1.9 copy-start.22
  191.8 1.9 copy-start.19
  191.8 2.0 copy-start.13
  193.9 3.8 %copy-start.3 = (bf16[480,2048]{1,0:T(8,128)(2,1)S(1)}, bf16[480,2048]{1,0:T(8,128)(2,1)}, u32[]{:S(2)}) copy-start(bf16[480,2048]{1,0:T(8,128)(2,1)} %copy-done.2) | copy-start | bytes 5898244
  193.9 3.8 %copy-start.10 = (f32[480,256]{1,0:T(8,128)S(1)}, f32[480,256]{1,0:T(8,128)}, u32[]{:S(2)}) copy-start(f32[480,256]{1,0:T(8,128)} %copy-done.9) | copy-start | bytes 1474564
  193.9 3.8 %copy-start.11 = (f32[480,256]{1,0:T(8,128)S(1)}, f32[480,256]{1,0:T(8,128)}, u32[]{:S(2)}) copy-start(f32[480,256]{1,0:T(8,128)} %fusion.7) | copy-start | bytes 1474564
  197.7 2.1 copy-start.23
  199.8 8.4 %copy-start.15 = (bf16[480,256]{1,0:T(8,128)(2,1)S(1)}, bf16[480,256]{1,0:T(8,128)(2,1)}, u32[]{:S(2)}) copy-start(bf16[480,256]{1,0:T(8,128)(2,1)} %copy-done.14) | copy-start | bytes 737284
  206.9 5.6 %collective-permute-start = (bf16[30,256]{1,0:T(8,128)(2,1)S(1)}, bf16[30,256]{1,0:T(8,128)(2,1)S(1)}, u32[]{:S(2)}, u32[]{:S(2)}) collective-permute-start(bf16[30,256]{1,0:T(8,128)(2,1)S(1)} %slice.37), channel_id=1, source_target_pairs={{4,0},{8,4},{12,8},{16,12},{20,16},{24,20},{28,24},{5,1},{9,5},{13... | collective-permute-start | bytes 46088 | tf_op jit(solution)/shard_map/ppermute | solution.py:12
  212.6 2.9 %copy-start.16 = (bf16[192,256]{1,0:T(8,128)(2,1)S(1)}, bf16[192,256]{1,0:T(8,128)(2,1)}, u32[]{:S(2)}) copy-start(bf16[192,256]{1,0:T(8,128)(2,1)} %param.28) | copy-start | bytes 294916
  212.6 2.9 %copy-start.17 = (bf16[192,256]{1,0:T(8,128)(2,1)S(1)}, bf16[192,256]{1,0:T(8,128)(2,1)}, u32[]{:S(2)}) copy-start(bf16[192,256]{1,0:T(8,128)(2,1)} %param.29) | copy-start | bytes 294916
Sparse Core Ops, SparseCore 0:
  40.7 21.5 all-gather.5
  71.1 21.6 all-gather.3
  100.9 30.3 reduce-scatter.2
  152.4 20.6 all-gather.7
  193.9 68.3 reduce-scatter.4
where the time goes:
time: 270 us; the launch traced here: 269 us
  waiting for transfers between devices  108 us (40%)
  blocking collectives  71.4 us (26%)
  local copies, waits for them, and re-layouts  39.8 us (15%)
  matrix products  24.5 us (9%)
  between operations  14.4 us (5%)
  other arithmetic  9.69 us (4%)
    reduce_scatter x1, waiting for transfers between devices, body(): lax.psum_scatter(contract_first(grad_stream, activated), 'sp', scatter_di...  46 us
    reduce_scatter x1, waiting for transfers between devices, body(): lax.psum_scatter(partial_rows.astype(jnp.bfloat16), 'tp', scatter_dimensi...  30.5 us
    all_to_all x1, blocking collectives, body(): lax.all_to_all(send_rows, 'sp', split_axis=0, concat_axis=0, tiled=True)  21.9 us
    all_to_all x1, blocking collectives, body(): lax.all_to_all(shared.reshape(experts, capacity, column), 'sp', split_axi...  19.8 us
    all_to_all x1, blocking collectives, body(): lax.all_to_all(send_cots, 'sp', split_axis=0, concat_axis=0, tiled=True)  17.4 us
    all_gather x1, waiting for transfers between devices, body(): lax.all_gather(got_cots, 'tp', axis=2, tiled=True)  15.8 us
    all_gather x1, waiting for transfers between devices, body(): back = lax.all_gather(back, 'tp', axis=2, tiled=True)  14.4 us
    dot_general x4, matrix products, contract_first(): lax.dot_general(left, right, (((0,), (0,)), ((), ())), preferred_element_...  11.4 us
  transfers between devices with their start and end apart: 6, of which 5 were waited for; matrix products, arithmetic and copies ran while one was open for 12% of the time, Pallas kernels for 0%

commit v1 on v0

v1 whole, which is shorter than its diff:
```python
import functools

import jax
import jax.numpy as jnp
from jax import lax
from jax.experimental import pallas as pl
from jax.experimental.pallas import tpu as pltpu
from jax.sharding import PartitionSpec as P

EPS = 1e-06
MESH = pl.DeviceIdType.MESH
F32 = jnp.float32
BF16 = jnp.bfloat16
HIGHEST = lax.Precision.HIGHEST


def silu_slope(value, sigma):
    return sigma * (1.0 + value * (1.0 - sigma))


def contract_last(left, right, precision=None):
    return lax.dot_general(
        left, right, (((1,), (1,)), ((), ())), preferred_element_type=F32, precision=precision
    )


def contract_first(left, right):
    return lax.dot_general(left, right, (((0,), (0,)), ((), ())), preferred_element_type=F32)


def round_up(value, unit):
    return -(-value // unit) * unit


def flip(index, mask):
    bit = 1
    while bit <= mask:
        if mask & bit:
            index = index + bit - 2 * bit * ((index // bit) % 2)
        bit *= 2
    return index


def low_bit(mask):
    return mask & -mask


def bits_below(limit):
    found, bit = [], 1
    while bit < limit:
        found.append(bit)
        bit *= 2
    return found[::-1]


def remote(src, dst, send, recv, where):
    return pltpu.make_async_remote_copy(
        src_ref=src, dst_ref=dst, send_sem=send, recv_sem=recv, device_id=where, device_id_type=MESH
    )


def enter(me, n, tp, groups):
    barrier = pltpu.get_barrier_semaphore()

    def greet(i, carry):
        pl.semaphore_signal(
            barrier, inc=1, device_id={"sp": lax.rem(me + i, n)}, device_id_type=MESH
        )
        return carry

    lax.fori_loop(1, n, greet, 0)
    for bit in bits_below(groups):
        pl.semaphore_signal(barrier, inc=1, device_id={"tp": flip(tp, bit)}, device_id_type=MESH)
    pl.semaphore_wait(barrier, n - 1 + len(bits_below(groups)))


class Spread:
    def __init__(self, place, tp, groups, send, recv):
        self.place, self.tp, self.groups = place, tp, groups
        self.send_sem, self.recv_sem = send, recv

    def copy(self, mask, bit):
        ref = self.place(flip(self.tp, mask))
        return remote(
            ref,
            ref,
            self.send_sem(mask | bit),
            self.recv_sem(mask | bit),
            {"tp": flip(self.tp, bit)},
        )

    def wait(self, mask):
        ref = self.place(flip(self.tp, mask))
        where = {"tp": flip(self.tp, low_bit(mask))}
        remote(ref, ref, self.send_sem(mask), self.recv_sem(mask), where).wait_recv()

    def begin(self):
        for bit in bits_below(self.groups):
            self.copy(0, bit).start()

    def masks(self):
        return sorted(range(1, self.groups), key=lambda m: (bin(m).count("1"), -low_bit(m)))

    def relay(self):
        for mask in self.masks():
            onward = bits_below(low_bit(mask))
            if onward:
                self.wait(mask)
                for bit in onward:
                    self.copy(mask, bit).start()

    def finish(self):
        for mask in self.masks():
            if not bits_below(low_bit(mask)):
                self.wait(mask)
        for mask in range(1, self.groups):
            self.copy(mask - low_bit(mask), low_bit(mask)).wait_send()


def each(first, last, step):
    def run(i, carry):
        step(i)
        return carry

    lax.fori_loop(first, last, run, 0)


def dispatch_kernel(
    n,
    groups,
    pcap,
    stream,
    upstream,
    gain,
    ids,
    weight,
    scores,
    filtered,
    rows,
    cots,
    places,
    stats,
    send_rows,
    send_cots,
    sp_send,
    sp_recv,
    tp_send,
    tp_recv,
    st_send,
    st_recv,
):
    me, tp = lax.axis_index("sp"), lax.axis_index("tp")
    tokens, width = stream.shape
    column = width // groups
    enter(me, n, tp, groups)

    filt = filtered[...]
    square = filt.astype(F32) * filt.astype(F32)
    high = square.astype(BF16)
    low = (square - high.astype(F32)).astype(BF16)
    ones = jnp.ones((8, filt.shape[1]), BF16)
    total = contract_last(ones, filt)
    total_square = contract_last(ones, high) + contract_last(ones, low)
    line = lax.broadcasted_iota(jnp.int32, total.shape, 0)
    stats[tp] = jnp.where(line == 0, total, total_square)
    sums = Spread(
        lambda o: stats.at[o], tp, groups, lambda m: st_send.at[m], lambda m: st_recv.at[m]
    )
    sums.begin()

    routes = 2 * tokens
    onehot = (lax.broadcasted_iota(jnp.int32, (n, routes), 0) == ids[...]).astype(F32)
    earlier = (
        lax.broadcasted_iota(jnp.int32, (routes, routes), 0)
        < lax.broadcasted_iota(jnp.int32, (routes, routes), 1)
    ).astype(F32).astype(BF16)
    before = jnp.dot(onehot.astype(BF16), earlier, preferred_element_type=F32)
    base = (lax.broadcasted_iota(jnp.int32, (n, routes), 0) * pcap).astype(F32)
    slot = jnp.sum(onehot * (before + base), axis=0, keepdims=True).astype(jnp.int32)
    slot_at = lax.broadcasted_iota(jnp.int32, (n * pcap, tokens), 0)
    first = (slot_at == slot[:, :tokens]).astype(F32).astype(BF16)
    second = (slot_at == slot[:, tokens:]).astype(F32).astype(BF16)
    both = first + second
    places[...] = both

    stream_f = stream[...].astype(F32)
    inv_rms = lax.rsqrt(jnp.mean(stream_f * stream_f, axis=1, keepdims=True) + EPS)
    cols = pl.ds(pl.multiple_of(tp * column, column), column)
    normed = (stream[:, cols].astype(F32) * inv_rms * gain[:, cols]).astype(BF16)
    send_rows[...] = jnp.dot(both, normed, preferred_element_type=F32).astype(BF16)
    spread = scores[:, 0:1] - scores[:, 1:2]
    up = upstream[:, cols].astype(F32)
    scaled_a = (weight[...] * jax.nn.sigmoid(spread) * up).astype(BF16)
    scaled_b = (weight[...] * jax.nn.sigmoid(-spread) * up).astype(BF16)
    send_cots[...] = (
        jnp.dot(first, scaled_a, preferred_element_type=F32)
        + jnp.dot(second, scaled_b, preferred_element_type=F32)
    ).astype(BF16)

    pairs = ((send_rows, rows), (send_cots, cots))

    def block(j):
        return pl.ds(pl.multiple_of(j * pcap, pcap), pcap)

    def place(full, s, o):
        return full.at[block(s), pl.ds(pl.multiple_of(o * column, column), column)]

    def sp_copy(a, i, j, s):
        src, full = pairs[a]
        return remote(
            src.at[block(j)], place(full, s, tp), sp_send.at[a, i], sp_recv.at[a, i], {"sp": j}
        )

    def send(i):
        for a in range(2):
            sp_copy(a, i, lax.rem(me + i, n), me).start()

    each(1, n, send)
    for src, full in pairs:
        full[block(me), cols] = src[block(me)]

    def gather(a, i):
        s = lax.rem(me + n - i, n)
        return Spread(
            lambda o: place(pairs[a][1], s, o),
            tp,
            groups,
            lambda m: tp_send.at[a, i, m],
            lambda m: tp_recv.at[a, i, m],
        )

    def arrive(i):
        for a in range(2):
            s = lax.rem(me + n - i, n)
            sp_copy(a, i, s, s).wait_recv()
            gather(a, i).begin()
            gather(a, i - 1).relay()

    for a in range(2):
        gather(a, 0).begin()
    each(1, n, arrive)
    for a in range(2):
        gather(a, n - 1).relay()
    sums.relay()
    sums.finish()

    def close(i):
        for a in range(2):
            gather(a, i).finish()

    each(0, n, close)

    def sent(i):
        for a in range(2):
            sp_copy(a, i, lax.rem(me + i, n), me).wait_send()

    each(1, n, sent)


def tail_kernel(
    n,
    groups,
    pcap,
    partial,
    places,
    stats,
    stream,
    upstream,
    gain,
    mixer,
    filtered,
    channel_gain,
    taps,
    value,
    gate,
    out_value,
    out_gating,
    out_mixer,
    halves,
    passing,
    keep,
    crossed,
    outgoing,
    back,
    grad_normed,
    grad_stream,
    staged,
    grad_all,
    act_all,
    slopes,
    halo_out,
    halo_in,
    ext,
    core_send,
    core_recv,
    x_send,
    x_recv,
    sp_send,
    sp_recv,
    gn_send,
    gn_recv,
    far_send,
    far_recv,
    near_send,
    near_recv,
    gs_send,
    gs_recv,
    ga_send,
    ga_recv,
    sl_send,
    sl_recv,
    halo_send,
    halo_recv,
):
    me, tp = lax.axis_index("sp"), lax.axis_index("tp")
    tokens, width = stream.shape
    column = width // groups
    channels = filtered.shape[1] * groups
    portion = tokens // groups
    db = width // n
    pdb = grad_all.shape[1]
    reach = taps.shape[0] - 1
    hpad = halo_in.shape[0]
    enter(me, n, tp, groups)

    def block(j):
        return pl.ds(pl.multiple_of(j * pcap, pcap), pcap)

    def quarter(q):
        return pl.ds(pl.multiple_of(q * column, column), column)

    mate = flip(tp, 1)
    half = groups // 2

    def chunk(i):
        return lax.rem(me + 1 + i, n)

    def core_copy(i, h):
        j = chunk(i)
        return remote(
            partial.at[block(j), quarter(lax.rem(mate, 2) + 2 * h)],
            halves.at[block(j), pl.ds(h * column, column)],
            core_send.at[i, h],
            core_recv.at[i, h],
            {"tp": mate},
        )

    def start_core(i):
        for h in range(half):
            core_copy(i, h).start()

    each(0, n, start_core)

    sums = stats[0]
    for o in range(1, groups):
        sums = sums + stats[o]
    eye = (
        lax.broadcasted_iota(jnp.int32, (tokens, tokens), 0)
        == lax.broadcasted_iota(jnp.int32, (tokens, tokens), 1)
    ).astype(F32)
    sums = contract_last(eye, sums, HIGHEST)
    mean_c = sums[:, 0:1] / channels
    variance = sums[:, 1:2] / channels - mean_c * mean_c
    inv_std = lax.rsqrt(variance + EPS)
    centred = (filtered[...].astype(F32) - mean_c) * inv_std
    normal_out = centred * channel_gain[...]
    sig_norm = jax.nn.sigmoid(normal_out)

    def act_rows(s):
        return pl.ds(pl.multiple_of(s * tokens, tokens), tokens)

    act_all[act_rows(me)] = (normal_out * sig_norm).astype(BF16)
    buddy = flip(me, 1)

    def far_copy(i, to, origin):
        ref = act_all.at[act_rows(origin)]
        return remote(ref, ref, far_send.at[i], far_recv.at[i], {"sp": to})

    def near_copy(i, holder):
        ref = act_all.at[act_rows(lax.rem(holder + n - 2 * i, n))]
        return remote(ref, ref, near_send.at[i], near_recv.at[i], {"sp": buddy})

    each(1, n // 2, lambda i: far_copy(i, lax.rem(me + 2 * i, n), me).start())
    near_copy(0, me).start()

    def x_copy(i, h):
        j = chunk(i)
        peer = lax.rem(tp, 2) + 2 * h
        ref = passing.at[block(j), pl.ds(h * column, column)]
        return peer, ref

    bits = [bit // 2 for bit in bits_below(groups) if bit > 1]
    mine = tp // 2

    def cross(i, m, wait):
        j = chunk(i)
        h = flip(mine, m)
        return remote(
            passing.at[block(j), pl.ds(pl.multiple_of(h * column, column), column)],
            crossed.at[block(j), pl.ds((m - 1) * column, column)],
            x_send.at[i, m],
            x_recv.at[i, m],
            {"tp": flip(tp, 2 * m)},
        )

    def add_core(i):
        j = chunk(i)
        for h in range(half):
            core_copy(i, h).wait_recv()
        for h in range(half):
            own = partial[block(j), quarter(lax.rem(tp, 2) + 2 * h)].astype(F32)
            passing[block(j), pl.ds(h * column, column)] = (
                own + halves[block(j), pl.ds(h * column, column)].astype(F32)
            ).astype(BF16)
        for m in range(1, half):
            cross(i, m, False).start()

    def home_copy(i, s):
        return remote(
            outgoing.at[block(chunk(i))],
            back.at[block(s)],
            sp_send.at[i],
            sp_recv.at[i],
            {"sp": chunk(i)},
        )

    def total_of(i):
        j = chunk(i)
        for m in range(1, half):
            cross(i, m, True).wait_recv()
        total = passing[block(j), pl.ds(pl.multiple_of(mine * column, column), column)].astype(F32)
        for m in range(1, half):
            total = total + crossed[block(j), pl.ds((m - 1) * column, column)].astype(F32)
        return total.astype(BF16)

    def add_x(i):
        outgoing[block(chunk(i))] = total_of(i)
        home_copy(i, me).start()

    add_core(0)

    def both(i):
        add_core(i)
        add_x(i - 1)

    each(1, n, both)
    back[block(me)] = total_of(n - 1)

    def relay_act(i):
        origin = lax.rem(me + n - 2 * i, n)
        far_copy(i, origin, origin).wait_recv()
        near_copy(i, me).start()

    each(1, n // 2, relay_act)

    inv_rms = jnp.zeros((tokens, 1), F32)
    for q in range(groups):
        piece = stream[:, q * column : (q + 1) * column].astype(F32)
        inv_rms = inv_rms + jnp.sum(piece * piece, axis=1, keepdims=True)
    inv_rms = lax.rsqrt(inv_rms / width + EPS)

    def came_home(i):
        s = lax.rem(me + n - 1 - i, n)
        home_copy(i, s).wait_recv()

    each(0, n - 1, came_home)
    grad_normed[:, quarter(tp)] = contract_first(places[...], back[...]).astype(BF16)
    gather = Spread(
        lambda o: grad_normed.at[:, quarter(o)],
        tp,
        groups,
        lambda m: gn_send.at[m],
        lambda m: gn_recv.at[m],
    )
    gather.begin()
    gather.relay()
    gather.finish()

    inner = jnp.zeros((tokens, 1), F32)
    for q in range(groups):
        at = slice(q * column, (q + 1) * column)
        weighted = grad_normed[:, at].astype(F32) * gain[:, at]
        inner = inner + jnp.sum(weighted * stream[:, at].astype(F32), axis=1, keepdims=True)
    inner = inv_rms * inv_rms * inv_rms * (inner / width)
    for q in range(groups):
        at = slice(q * column, (q + 1) * column)
        weighted = grad_normed[:, at].astype(F32) * gain[:, at]
        grad_stream[:, at] = (
            upstream[:, at].astype(F32) + inv_rms * weighted - stream[:, at].astype(F32) * inner
        ).astype(BF16)

    def part(s, o):
        start = pl.multiple_of(s * tokens + o * portion, portion)
        return grad_all.at[pl.ds(start, portion)]

    my_rows = pl.ds(pl.multiple_of(tp * portion, portion), portion)
    if db == pdb:

        def cut(j):
            return grad_stream.at[my_rows, pl.ds(pl.multiple_of(j * db, db), db)]

        grad_all[act_rows(me)] = grad_stream[:, pl.ds(pl.multiple_of(me * db, db), db)]
    else:

        def pick(j):
            where = lax.broadcasted_iota(jnp.int32, (width, pdb), 0)
            lane = lax.broadcasted_iota(jnp.int32, (width, pdb), 1)
            return ((where == lane + j * db) & (lane < db)).astype(F32).astype(BF16)

        def stage(j):
            staged[j] = jnp.dot(
                grad_stream[my_rows], pick(j), preferred_element_type=F32
            ).astype(BF16)

        each(0, n, stage)

        def cut(j):
            return staged.at[j]

        grad_all[act_rows(me)] = jnp.dot(
            grad_stream[...], pick(me), preferred_element_type=F32
        ).astype(BF16)

    def cut_copy(i, j, s):
        return remote(cut(j), part(s, tp), gs_send.at[i], gs_recv.at[i], {"sp": j})

    each(1, n, lambda i: cut_copy(i, lax.rem(me + i, n), me).start())

    grad_act = contract_last(grad_stream[...], mixer[...])
    grad_centred = grad_act * silu_slope(normal_out, sig_norm) * channel_gain[...]
    ones = jnp.ones((8, filtered.shape[1]), F32)
    slope_sum = contract_last(ones, grad_centred, HIGHEST)
    slope_cross = contract_last(ones, grad_centred * centred, HIGHEST)
    line = lax.broadcasted_iota(jnp.int32, slope_sum.shape, 0)
    slopes[tp] = jnp.where(line == 0, slope_sum, slope_cross)
    meet = Spread(
        lambda o: slopes.at[o], tp, groups, lambda m: sl_send.at[m], lambda m: sl_recv.at[m]
    )
    meet.begin()
    meet.relay()
    meet.finish()
    sums = slopes[0]
    for o in range(1, groups):
        sums = sums + slopes[o]
    sums = contract_last(eye, sums, HIGHEST)
    grad_filtered = (
        inv_std
        * (grad_centred - sums[:, 0:1] / channels - centred * (sums[:, 1:2] / channels))
    ).astype(BF16)
    halo_out[...] = grad_filtered[:hpad]
    ext[:tokens] = grad_filtered.astype(F32)

    def halo_copy():
        return remote(halo_out, halo_in, halo_send, halo_recv, {"sp": lax.rem(me + n - 1, n)})

    halo_copy().start()

    def spread_cut(i):
        s = lax.rem(me + n - i, n)
        return Spread(
            lambda o: part(s, o),
            tp,
            groups,
            lambda m: ga_send.at[i, m],
            lambda m: ga_recv.at[i, m],
        )

    def cut_arrives(i):
        s = lax.rem(me + n - i, n)
        cut_copy(i, s, s).wait_recv()
        spread_cut(i).begin()

    each(1, n, cut_arrives)

    halo_copy().wait_recv()
    inside = jnp.where(me < n - 1, 1.0, 0.0)
    ext[tokens:] = halo_in[...].astype(F32) * inside
    each(1, n, lambda i: spread_cut(i).relay())
    mixed = jnp.zeros((tokens, filtered.shape[1]), F32)
    for k in range(reach + 1):
        mixed = mixed + taps[k : k + 1] * ext[reach - k : reach - k + tokens]
    sig_gate = jax.nn.sigmoid(gate[...].astype(F32))
    out_value[...] = (mixed * sig_gate).astype(BF16)
    out_gating[...] = (mixed * value[...].astype(F32) * sig_gate * (1.0 - sig_gate)).astype(BF16)

    each(1, n, lambda i: spread_cut(i).finish())
    each(0, n // 2, lambda i: near_copy(i, buddy).wait_recv())
    out_mixer[...] = contract_first(grad_all[...], act_all[...])[:db]

    halo_copy().wait_send()
    each(1, n, lambda i: cut_copy(i, lax.rem(me + i, n), me).wait_send())
    each(1, n // 2, lambda i: far_copy(i, lax.rem(me + 2 * i, n), me).wait_send())
    each(0, n // 2, lambda i: near_copy(i, me).wait_send())
    each(0, n - 1, lambda i: home_copy(i, me).wait_send())

    def sums_sent(i):
        for h in range(half):
            core_copy(i, h).wait_send()
        for m in range(1, half):
            cross(i, m, True).wait_send()

    each(0, n, sums_sent)


def call(kernel, collective_id, outs, scratch, args):
    return pl.pallas_call(
        kernel,
        out_shape=outs,
        in_specs=[pl.BlockSpec(memory_space=pltpu.VMEM)] * len(args),
        out_specs=[pl.BlockSpec(memory_space=pltpu.VMEM)] * len(outs),
        scratch_shapes=scratch,
        compiler_params=pltpu.CompilerParams(
            collective_id=collective_id, has_side_effects=True, vmem_limit_bytes=40 << 20
        ),
    )(*args)


def body(
    stream,
    upstream,
    expert_gain,
    expert_ids,
    group_weight,
    pair_scores,
    gate_weight,
    up_weight,
    down_weight,
    mixer_weight,
    filtered,
    channel_gain,
    kernel_taps,
    value_branch,
    gate_branch,
):
    n, groups = lax.axis_size("sp"), lax.axis_size("tp")
    tokens, width = stream.shape
    capacity = max(2, 5 * tokens // (2 * n))
    pcap = round_up(capacity, 16)
    column = width // groups
    here = filtered.shape[1]
    slots = n * pcap
    dma = pltpu.SemaphoreType.DMA
    shape = jax.ShapeDtypeStruct
    gain = expert_gain[None]
    rows, cots, places, stats = call(
        functools.partial(dispatch_kernel, n, groups, pcap),
        0,
        [
            shape((slots, width), BF16),
            shape((slots, width), BF16),
            shape((slots, tokens), BF16),
            shape((groups, 8, tokens), F32),
        ],
        [
            pltpu.VMEM((slots, column), BF16),
            pltpu.VMEM((slots, column), BF16),
            dma((2, n)),
            dma((2, n)),
            dma((2, n, groups)),
            dma((2, n, groups)),
            dma((groups,)),
            dma((groups,)),
        ],
        (
            stream,
            upstream,
            gain,
            expert_ids.T.reshape(1, 2 * tokens),
            group_weight[:, None],
            pair_scores,
            filtered,
        ),
    )
    gate_local, up_local, down_local = gate_weight[0], up_weight[0], down_weight[0]
    pre_gate = jnp.dot(rows, gate_local, preferred_element_type=F32)
    pre_up = jnp.dot(rows, up_local, preferred_element_type=F32)
    sigma = jax.nn.sigmoid(pre_gate)
    silu_gate = pre_gate * sigma
    hidden = (silu_gate * pre_up).astype(BF16)
    grad_hidden = contract_last(cots, down_local)
    grad_pre_gate = (grad_hidden * pre_up * silu_slope(pre_gate, sigma)).astype(BF16)
    grad_pre_up = (grad_hidden * silu_gate).astype(BF16)
    partial = (
        contract_last(grad_pre_gate, gate_local) + contract_last(grad_pre_up, up_local)
    ).astype(BF16)
    gradient_gate = contract_first(rows, grad_pre_gate)[None]
    gradient_up = contract_first(rows, grad_pre_up)[None]
    gradient_down = contract_first(hidden, cots)[None]
    db = width // n
    pdb = round_up(db, 128)
    half = groups // 2
    hpad = round_up(kernel_taps.shape[0] - 1, 16)
    staged = (n, tokens // groups, pdb) if pdb != db else (1, 16, 128)
    gradient_value, gradient_gating, gradient_mixer = call(
        functools.partial(tail_kernel, n, groups, pcap),
        1,
        [
            shape((tokens, here), BF16),
            shape((tokens, here), BF16),
            shape((db, here), F32),
        ],
        [
            pltpu.VMEM((slots, half * column), BF16),
            pltpu.VMEM((slots, half * column), BF16),
            pltpu.VMEM((16, 128), F32),
            pltpu.VMEM((slots, max(1, half - 1) * column), BF16),
            pltpu.VMEM((slots, column), BF16),
            pltpu.VMEM((slots, column), BF16),
            pltpu.VMEM((tokens, width), BF16),
            pltpu.VMEM((tokens, width), BF16),
            pltpu.VMEM(staged, BF16),
            pltpu.VMEM((n * tokens, pdb), BF16),
            pltpu.VMEM((n * tokens, here), BF16),
            pltpu.VMEM((groups, 8, tokens), F32),
            pltpu.VMEM((hpad, here), BF16),
            pltpu.VMEM((hpad, here), BF16),
            pltpu.VMEM((tokens + hpad, here), F32),
            dma((n, half)),
            dma((n, half)),
            dma((n, half)),
            dma((n, half)),
            dma((n,)),
            dma((n,)),
            dma((groups,)),
            dma((groups,)),
            dma((n // 2,)),
            dma((n // 2,)),
            dma((n // 2,)),
            dma((n // 2,)),
            dma((n,)),
            dma((n,)),
            dma((n, groups)),
            dma((n, groups)),
            dma((groups,)),
            dma((groups,)),
            dma(()),
            dma(()),
        ],
        (
            partial,
            places,
            stats,
            stream,
            upstream,
            gain,
            mixer_weight,
            filtered,
            channel_gain[None],
            kernel_taps,
            value_branch,
            gate_branch,
        ),
    )
    return (
        gradient_value,
        gradient_gating,
        gradient_mixer,
        gradient_gate,
        gradient_up,
        gradient_down,
    )


def solution(mesh):
    return jax.shard_map(
        body,
        mesh=mesh,
        in_specs=(
            P("sp", None),
            P("sp", None),
            P(),
            P("sp", None),
            P("sp"),
            P("sp", None),
            P("sp", None, "tp"),
            P("sp", None, "tp"),
            P("sp", "tp", None),
            P("tp", None),
            P("sp", "tp"),
            P("tp"),
            P(None, "tp"),
            P("sp", "tp"),
            P("sp", "tp"),
        ),
        out_specs=(
            P("sp", "tp"),
            P("sp", "tp"),
            P("sp", "tp"),
            P("sp", None, "tp"),
            P("sp", None, "tp"),
            P("sp", "tp", None),
        ),
        check_vma=False,
    )
```

time: 270 us -> 112 us (0.41)
  waiting for transfers between devices: 108 us -> 0 us
  Pallas kernels: 0 us -> 91.4 us
  blocking collectives: 71.4 us -> 0 us
  local copies, waits for them, and re-layouts: 39.8 us -> 9.75 us
  matrix products: 24.5 us -> 10 us
  between operations: 14.4 us -> 0.78 us
  other arithmetic: 9.69 us -> 0 us
    pallas_call x0 -> x2, Pallas kernels: none -> 91.4 us  [call(): pl.pallas_call(kernel, out_shape=outs, in_specs=[pl.BlockSpec(memory_spac...]
    reduce_scatter x2 -> x0, waiting for transfers between devices: 76.5 us -> none  [the longest x1 46 us: body(): lax.psum_scatter(contract_first(grad_stream, activated), 'sp', scatter_di...]
    all_to_all x3 -> x0, blocking collectives: 59 us -> none  [the longest x1 21.9 us: body(): lax.all_to_all(send_rows, 'sp', split_axis=0, concat_axis=0, tiled=True)]
    all_gather x3 -> x0, waiting for transfers between devices: 30.3 us -> none  [the longest x1 15.8 us: body(): lax.all_gather(got_cots, 'tp', axis=2, tiled=True)]
    psum x2 -> x0, blocking collectives: 12.4 us -> none  [the longest x1 6.29 us: body(): lax.psum((jnp.sum(grad_centred, axis=1), jnp.sum(grad_centred * centred,...]
    mul x6 -> x0, local copies, waits for them, and re-layouts: 9.32 us -> none  [the longest x2 8.83 us: body(): route_weight[:, :, None] * upstream.astype(jnp.float32)[:, None, :]]
    gather x3 -> x0, local copies, waits for them, and re-layouts: 7.37 us -> none  [the longest x1 3.11 us: body(): back_flat[slots].astype(jnp.float32).reshape(tokens_here, 2, width)]
    slice x3 -> x0, local copies, waits for them, and re-layouts: 6.36 us -> none  [the longest x1 6.14 us: body(): grad_normed = per_route[:, 0] + per_route[:, 1]]
  transfers between devices with their start and end apart: 6 -> 0, of which waited for: 5 -> 0; matrix products, arithmetic and copies ran while one was open for 12% -> 0% of each run, Pallas kernels for 0% -> 0%
where the time goes in v1:
time: 112 us
  Pallas kernels  91.4 us (82%)
  matrix products  10 us (9%)
  local copies, waits for them, and re-layouts  9.75 us (9%)
    pallas_call x2, Pallas kernels, call(): pl.pallas_call(kernel, out_shape=outs, in_specs=[pl.BlockSpec(memory_spac...  91.4 us
    unnamed x30, local copies, waits for them, and re-layouts  8.1 us
    dot_general x3, matrix products, contract_first(): lax.dot_general(left, right, (((0,), (0,)), ((), ())), preferred_element_...  6.23 us
    dot_general x3, matrix products, contract_last(): lax.dot_general(left, right, (((1,), (1,)), ((), ())), preferred_element_...  2.37 us

profile of v1, /device:TPU:0, one launch (start us, length us, event | category | flops | bytes accessed | tf_op | source)
XLA Modules:
  0.0 112.0 jit_solution(7489124272304244496)
XLA Ops:
  0.6 0.0 copy-start
  0.6 0.9 copy.22.weight
  1.5 0.8 copy.23.scores
  2.3 0.8 reshape.15.ids
  3.1 0.0 copy-start.1
  3.1 1.1 %copy-done.1 = bf16[192,2048]{1,0:T(8,128)(2,1)S(1)} copy-done((bf16[192,2048]{1,0:T(8,128)(2,1)S(1)}, bf16[192,2048]{1,0:T(8,128)(2,1)}, u32[]{:S(2)}) %copy-start.1) | copy-done | bytes 786456
  4.2 0.0 copy-start.2
  4.2 1.1 %copy-done.2 = bf16[192,2048]{1,0:T(8,128)(2,1)S(1)} copy-done((bf16[192,2048]{1,0:T(8,128)(2,1)S(1)}, bf16[192,2048]{1,0:T(8,128)(2,1)}, u32[]{:S(2)}) %copy-start.2) | copy-done | bytes 786456
  5.4 0.0 copy-start.4
  5.4 0.9 copy-done.4
  6.3 0.0 copy-start.9
  6.3 0.7 copy-done.9
  7.0 40.2 %shard_map.190 = (bf16[512,2048]{1,0:T(8,128)(2,1)S(1)}, bf16[512,2048]{1,0:T(8,128)(2,1)S(1)}, bf16[512,192]{1,0:T(8,128)(2,1)S(1)}, f32[4,8,192]{2,1,0:T(8,128)S(1)}) custom-call(bf16[192,2048]{1,0:T(8,128)(2,1)S(1)} %copy-done.1, bf16[192,2048]{1,0:T(8,128)(2,1)S(1)} %copy-done.2, f32[1,2048]{1,0:T(1,128)S(1)} %bitcast.35, s32[1,384]{1,0:T(1,128)S(1)} %reshape.15.ids, ...), custom_call_target="tpu_custom_call" | custom-call | tf_op jit(solution)/shard_map/pallas_call | solution.py:606
  47.2 0.0 copy-start.11
  47.2 0.0 copy-done
  47.2 0.7 fusion.2
  47.9 0.5 copy-done.11
  48.4 0.0 copy-start.12
  48.4 0.7 fusion.5
  49.1 0.5 copy-done.12
  49.6 0.9 multiply_convert_fusion.1
  50.5 0.7 fusion
  51.2 0.0 copy-start.3
  51.3 0.0 copy-start.5
  51.3 0.0 copy-start.6
  51.3 0.0 copy-start.7
  51.3 0.0 copy-start.8
  51.3 0.0 copy-start.10
  51.3 0.7 add_convert_fusion.partial
  52.1 0.4 copy-done.3
  52.5 0.0 copy-done.5
  52.5 0.0 copy-done.6
  52.5 0.0 copy-done.7
  52.5 0.0 copy-done.8
  52.5 0.0 copy-done.10
  52.5 51.2 %shard_map.191 = (bf16[192,256]{1,0:T(8,128)(2,1)S(1)}, bf16[192,256]{1,0:T(8,128)(2,1)S(1)}, f32[256,256]{1,0:T(8,128)S(1)}) custom-call(bf16[512,2048]{1,0:T(8,128)(2,1)S(1)} %add_convert_fusion.partial, bf16[512,192]{1,0:T(8,128)(2,1)S(1)} %get-tuple-element.15.places, f32[4,8,192]{2,1,0:T(8,128)S(1)} %get-tuple-element.16.stats, ...), custom_call_target="tpu_custom_call" | custom-call | tf_op jit(solution)/shard_map/pallas_call | solution.py:606
  103.7 2.1 %convolution_bitcast_fusion.1 = f32[1,2048,256]{2,1,0:T(8,128)} fusion(bf16[512,2048]{1,0:T(8,128)(2,1)S(1)} %get-tuple-element.14, bf16[512,256]{1,0:T(8,128)(2,1)S(1)} %get-tuple-element.20), kind=kOutput, calls=%fused_computation.2 | convolution fusion | flops 536870912 | bytes 4456448 | tf_op jit(solution)/shard_map/dot_general | solution.py:28
  105.8 2.1 %convolution_bitcast_fusion.2 = f32[1,2048,256]{2,1,0:T(8,128)} fusion(bf16[512,2048]{1,0:T(8,128)(2,1)S(1)} %get-tuple-element.14, bf16[512,256]{1,0:T(8,128)(2,1)S(1)} %get-tuple-element.21), kind=kOutput, calls=%fused_computation.3 | convolution fusion | flops 536870912 | bytes 4456448 | tf_op jit(solution)/shard_map/dot_general | solution.py:28
  107.9 2.1 %convolution_bitcast_fusion = f32[1,256,2048]{2,1,0:T(8,128)} fusion(bf16[512,2048]{1,0:T(8,128)(2,1)S(1)} %get-tuple-element.13, f32[512,256]{1,0:T(8,128)S(1)} %fusion.5, f32[512,256]{1,0:T(8,128)S(1)} %fusion.2), kind=kOutput, calls=%fused_computation.1 | convolution fusion | flops 537657344 | bytes 5242880 | tf_op jit(solution)/shard_map/dot_general | solution.py:28
  110.0 0.6 copy.27
  110.6 0.6 copy.28
  111.3 0.7 copy.29
Async XLA Ops:
  0.6 46.5 %copy-start = (bf16[1,2048,256]{2,1,0:T(8,128)(2,1)S(1)}, bf16[1,2048,256]{2,1,0:T(8,128)(2,1)}, u32[]{:S(2)}) copy-start(bf16[1,2048,256]{2,1,0:T(8,128)(2,1)} %param.21) | copy-start | bytes 3145732
  3.1 1.1 %copy-start.1 = (bf16[192,2048]{1,0:T(8,128)(2,1)S(1)}, bf16[192,2048]{1,0:T(8,128)(2,1)}, u32[]{:S(2)}) copy-start(bf16[192,2048]{1,0:T(8,128)(2,1)} %stream.3) | copy-start | bytes 2359300
  4.2 1.1 %copy-start.2 = (bf16[192,2048]{1,0:T(8,128)(2,1)S(1)}, bf16[192,2048]{1,0:T(8,128)(2,1)}, u32[]{:S(2)}) copy-start(bf16[192,2048]{1,0:T(8,128)(2,1)} %upstream.3) | copy-start | bytes 2359300
  5.4 0.9 copy-start.4
  6.3 0.7 copy-start.9
  47.2 1.2 %copy-start.11 = (bf16[1,2048,256]{2,1,0:T(8,128)(2,1)S(1)}, bf16[1,2048,256]{2,1,0:T(8,128)(2,1)}, u32[]{:S(2)}) copy-start(bf16[1,2048,256]{2,1,0:T(8,128)(2,1)} %param.22) | copy-start | bytes 3145732
  48.4 1.2 %copy-start.12 = (bf16[1,256,2048]{2,1,0:T(8,128)(2,1)S(1)}, bf16[1,256,2048]{2,1,0:T(8,128)(2,1)}, u32[]{:S(2)}) copy-start(bf16[1,256,2048]{2,1,0:T(8,128)(2,1)} %param.23) | copy-start | bytes 3145732
  51.2 1.2 %copy-start.3 = (bf16[256,2048]{1,0:T(8,128)(2,1)S(1)}, bf16[256,2048]{1,0:T(8,128)(2,1)}, u32[]{:S(2)}) copy-start(bf16[256,2048]{1,0:T(8,128)(2,1)} %mixer.1) | copy-start | bytes 3145732
  51.3 1.2 %copy-start.5 = (bf16[192,256]{1,0:T(8,128)(2,1)S(1)}, bf16[192,256]{1,0:T(8,128)(2,1)}, u32[]{:S(2)}) copy-start(bf16[192,256]{1,0:T(8,128)(2,1)} %filtered.3) | copy-start | bytes 294916
  51.3 1.2 %copy-start.6 = (bf16[192,256]{1,0:T(8,128)(2,1)S(1)}, bf16[192,256]{1,0:T(8,128)(2,1)}, u32[]{:S(2)}) copy-start(bf16[192,256]{1,0:T(8,128)(2,1)} %value.1) | copy-start | bytes 294916
  51.3 1.2 %copy-start.7 = (bf16[192,256]{1,0:T(8,128)(2,1)S(1)}, bf16[192,256]{1,0:T(8,128)(2,1)}, u32[]{:S(2)}) copy-start(bf16[192,256]{1,0:T(8,128)(2,1)} %gate.1) | copy-start | bytes 294916
  51.3 1.2 %copy-start.8 = (f32[31,256]{1,0:T(8,128)S(1)}, f32[31,256]{1,0:T(8,128)}, u32[]{:S(2)}) copy-start(f32[31,256]{1,0:T(8,128)} %taps.1) | copy-start | bytes 95236
  51.3 1.2 %copy-start.10 = (f32[256]{0:T(256)S(1)}, f32[256]{0:T(256)}, u32[]{:S(2)}) copy-start(f32[256]{0:T(256)} %param.26) | copy-start | bytes 3076

commit v2 on v1

--- a/solution.py
+++ b/solution.py
@@ -215,7 +215,8 @@
         for a in range(2):
             sp_copy(a, i, lax.rem(me + i, n), me).start()
 
-    each(1, n, send)
+    window = min(n - 1, 3)
+    each(1, window + 1, send)
     for src, full in pairs:
         full[block(me), cols] = src[block(me)]
 
@@ -233,6 +234,8 @@
         for a in range(2):
             s = lax.rem(me + n - i, n)
             sp_copy(a, i, s, s).wait_recv()
+            if a == 0:
+                pl.when(i + window < n)(lambda: send(i + window))
             gather(a, i).begin()
             gather(a, i - 1).relay()
 

time: 112 us -> 112 us (level)
  no operation moved by 1% of the time
where the time goes in v2:
time: 112 us
  Pallas kernels  91.4 us (82%)
  matrix products  10 us (9%)
  local copies, waits for them, and re-layouts  9.75 us (9%)
    pallas_call x2, Pallas kernels, call(): pl.pallas_call(kernel, out_shape=outs, in_specs=[pl.BlockSpec(memory_spac...  91.4 us
    unnamed x30, local copies, waits for them, and re-layouts  8.1 us
    dot_general x3, matrix products, contract_first(): lax.dot_general(left, right, (((0,), (0,)), ((), ())), preferred_element_...  6.22 us
    dot_general x3, matrix products, contract_last(): lax.dot_general(left, right, (((1,), (1,)), ((), ())), preferred_element_...  2.37 us

profile of v2, /device:TPU:0, one launch (start us, length us, event | category | flops | bytes accessed | tf_op | source)
XLA Modules:
  0.0 111.9 jit_solution(1085850886223859714)
XLA Ops:
  0.6 0.0 copy-start
  0.6 0.9 copy.22.weight
  1.5 0.8 copy.23.scores
  2.3 0.8 reshape.15.ids
  3.1 0.0 copy-start.1
  3.1 1.1 %copy-done.1 = bf16[192,2048]{1,0:T(8,128)(2,1)S(1)} copy-done((bf16[192,2048]{1,0:T(8,128)(2,1)S(1)}, bf16[192,2048]{1,0:T(8,128)(2,1)}, u32[]{:S(2)}) %copy-start.1) | copy-done | bytes 786456
  4.2 0.0 copy-start.2
  4.2 1.1 %copy-done.2 = bf16[192,2048]{1,0:T(8,128)(2,1)S(1)} copy-done((bf16[192,2048]{1,0:T(8,128)(2,1)S(1)}, bf16[192,2048]{1,0:T(8,128)(2,1)}, u32[]{:S(2)}) %copy-start.2) | copy-done | bytes 786456
  5.4 0.0 copy-start.4
  5.4 0.9 copy-done.4
  6.3 0.0 copy-start.9
  6.3 0.7 copy-done.9
  7.0 40.1 %shard_map.190 = (bf16[512,2048]{1,0:T(8,128)(2,1)S(1)}, bf16[512,2048]{1,0:T(8,128)(2,1)S(1)}, bf16[512,192]{1,0:T(8,128)(2,1)S(1)}, f32[4,8,192]{2,1,0:T(8,128)S(1)}) custom-call(bf16[192,2048]{1,0:T(8,128)(2,1)S(1)} %copy-done.1, bf16[192,2048]{1,0:T(8,128)(2,1)S(1)} %copy-done.2, f32[1,2048]{1,0:T(1,128)S(1)} %bitcast.35, s32[1,384]{1,0:T(1,128)S(1)} %reshape.15.ids, ...), custom_call_target="tpu_custom_call" | custom-call | tf_op jit(solution)/shard_map/pallas_call | solution.py:609
  47.1 0.0 copy-start.11
  47.1 0.0 copy-done
  47.1 0.7 fusion.2
  47.8 0.5 copy-done.11
  48.3 0.0 copy-start.12
  48.3 0.7 fusion.5
  49.0 0.5 copy-done.12
  49.5 0.9 multiply_convert_fusion.1
  50.4 0.7 fusion
  51.2 0.0 copy-start.3
  51.2 0.0 copy-start.5
  51.2 0.0 copy-start.6
  51.2 0.0 copy-start.7
  51.2 0.0 copy-start.8
  51.2 0.0 copy-start.10
  51.2 0.7 add_convert_fusion.partial
  52.0 0.4 copy-done.3
  52.4 0.0 copy-done.5
  52.4 0.0 copy-done.6
  52.4 0.0 copy-done.7
  52.4 0.0 copy-done.8
  52.4 0.0 copy-done.10
  52.4 51.3 %shard_map.191 = (bf16[192,256]{1,0:T(8,128)(2,1)S(1)}, bf16[192,256]{1,0:T(8,128)(2,1)S(1)}, f32[256,256]{1,0:T(8,128)S(1)}) custom-call(bf16[512,2048]{1,0:T(8,128)(2,1)S(1)} %add_convert_fusion.partial, bf16[512,192]{1,0:T(8,128)(2,1)S(1)} %get-tuple-element.15.places, f32[4,8,192]{2,1,0:T(8,128)S(1)} %get-tuple-element.16.stats, ...), custom_call_target="tpu_custom_call" | custom-call | tf_op jit(solution)/shard_map/pallas_call | solution.py:609
  103.7 2.1 %convolution_bitcast_fusion.1 = f32[1,2048,256]{2,1,0:T(8,128)} fusion(bf16[512,2048]{1,0:T(8,128)(2,1)S(1)} %get-tuple-element.14, bf16[512,256]{1,0:T(8,128)(2,1)S(1)} %get-tuple-element.20), kind=kOutput, calls=%fused_computation.2 | convolution fusion | flops 536870912 | bytes 4456448 | tf_op jit(solution)/shard_map/dot_general | solution.py:28
  105.8 2.1 %convolution_bitcast_fusion.2 = f32[1,2048,256]{2,1,0:T(8,128)} fusion(bf16[512,2048]{1,0:T(8,128)(2,1)S(1)} %get-tuple-element.14, bf16[512,256]{1,0:T(8,128)(2,1)S(1)} %get-tuple-element.21), kind=kOutput, calls=%fused_computation.3 | convolution fusion | flops 536870912 | bytes 4456448 | tf_op jit(solution)/shard_map/dot_general | solution.py:28
  107.8 2.1 %convolution_bitcast_fusion = f32[1,256,2048]{2,1,0:T(8,128)} fusion(bf16[512,2048]{1,0:T(8,128)(2,1)S(1)} %get-tuple-element.13, f32[512,256]{1,0:T(8,128)S(1)} %fusion.5, f32[512,256]{1,0:T(8,128)S(1)} %fusion.2), kind=kOutput, calls=%fused_computation.1 | convolution fusion | flops 537657344 | bytes 5242880 | tf_op jit(solution)/shard_map/dot_general | solution.py:28
  109.9 0.6 copy.27
  110.6 0.6 copy.28
  111.2 0.7 copy.29
Async XLA Ops:
  0.6 46.5 %copy-start = (bf16[1,2048,256]{2,1,0:T(8,128)(2,1)S(1)}, bf16[1,2048,256]{2,1,0:T(8,128)(2,1)}, u32[]{:S(2)}) copy-start(bf16[1,2048,256]{2,1,0:T(8,128)(2,1)} %param.21) | copy-start | bytes 3145732
  3.1 1.1 %copy-start.1 = (bf16[192,2048]{1,0:T(8,128)(2,1)S(1)}, bf16[192,2048]{1,0:T(8,128)(2,1)}, u32[]{:S(2)}) copy-start(bf16[192,2048]{1,0:T(8,128)(2,1)} %stream.3) | copy-start | bytes 2359300
  4.2 1.1 %copy-start.2 = (bf16[192,2048]{1,0:T(8,128)(2,1)S(1)}, bf16[192,2048]{1,0:T(8,128)(2,1)}, u32[]{:S(2)}) copy-start(bf16[192,2048]{1,0:T(8,128)(2,1)} %upstream.3) | copy-start | bytes 2359300
  5.4 0.9 copy-start.4
  6.3 0.7 copy-start.9
  47.1 1.2 %copy-start.11 = (bf16[1,2048,256]{2,1,0:T(8,128)(2,1)S(1)}, bf16[1,2048,256]{2,1,0:T(8,128)(2,1)}, u32[]{:S(2)}) copy-start(bf16[1,2048,256]{2,1,0:T(8,128)(2,1)} %param.22) | copy-start | bytes 3145732
  48.3 1.2 %copy-start.12 = (bf16[1,256,2048]{2,1,0:T(8,128)(2,1)S(1)}, bf16[1,256,2048]{2,1,0:T(8,128)(2,1)}, u32[]{:S(2)}) copy-start(bf16[1,256,2048]{2,1,0:T(8,128)(2,1)} %param.23) | copy-start | bytes 3145732
  51.2 1.2 %copy-start.3 = (bf16[256,2048]{1,0:T(8,128)(2,1)S(1)}, bf16[256,2048]{1,0:T(8,128)(2,1)}, u32[]{:S(2)}) copy-start(bf16[256,2048]{1,0:T(8,128)(2,1)} %mixer.1) | copy-start | bytes 3145732
  51.2 1.2 %copy-start.5 = (bf16[192,256]{1,0:T(8,128)(2,1)S(1)}, bf16[192,256]{1,0:T(8,128)(2,1)}, u32[]{:S(2)}) copy-start(bf16[192,256]{1,0:T(8,128)(2,1)} %filtered.3) | copy-start | bytes 294916
  51.2 1.2 %copy-start.6 = (bf16[192,256]{1,0:T(8,128)(2,1)S(1)}, bf16[192,256]{1,0:T(8,128)(2,1)}, u32[]{:S(2)}) copy-start(bf16[192,256]{1,0:T(8,128)(2,1)} %value.1) | copy-start | bytes 294916
  51.2 1.2 %copy-start.7 = (bf16[192,256]{1,0:T(8,128)(2,1)S(1)}, bf16[192,256]{1,0:T(8,128)(2,1)}, u32[]{:S(2)}) copy-start(bf16[192,256]{1,0:T(8,128)(2,1)} %gate.1) | copy-start | bytes 294916
  51.2 1.2 %copy-start.8 = (f32[31,256]{1,0:T(8,128)S(1)}, f32[31,256]{1,0:T(8,128)}, u32[]{:S(2)}) copy-start(f32[31,256]{1,0:T(8,128)} %taps.1) | copy-start | bytes 95236
  51.2 1.2 %copy-start.10 = (f32[256]{0:T(256)S(1)}, f32[256]{0:T(256)}, u32[]{:S(2)}) copy-start(f32[256]{0:T(256)} %param.26) | copy-start | bytes 3076
